TPU v7x, 512 devices: a whole 4x4x16 slice. The times are simulated.
512 devices in a mesh: ep: 16 (over y, x), tp: 32 (over z, core).
Axes of the slice: x: 4, y: 4, z: 16, core: 2. Of those that a mesh axis runs over, the one named last changes fastest.
Arguments:
- features: bfloat16 [256, 1024], P('ep', 'tp'), may hold values from -6 to 6
- key_table: bfloat16 [262144, 1024], P('ep', 'tp'), may hold values from -0.1875 to 0.1875
- value_table: bfloat16 [262144, 1024], P('ep', 'tp'), may hold values from -6 to 6
- chosen: int32 [256, 4, 16], P('ep'), may hold values from 0 to 262143
- scores: float32 [256, 4, 16], P('ep'), may hold values from -8 to 8
Outputs:
- mixed: bfloat16 [256, 1024], P('ep', 'tp')
Inputs may be any that keep to these rules, and one draw needn't show every extreme that they name: Every chosen row is a row of the tables, 0 to 262143; rows may repeat, and a few rows are far more popular than the rest.
All inputs are finite; a program needn't handle non-finite values.
Results may differ from a plain program's by a relative error of at most 0.0065.
Values may be sent and summed in bfloat16 or wider, within the bound.
A program may use at most 64 MiB of HBM per device.

v0:
```python
import functools

import jax
import jax.numpy as jnp
from jax import lax
from jax.experimental import pallas as pl
from jax.experimental.pallas import tpu as pltpu
from jax.sharding import PartitionSpec as P

LANES = 128
GROUP = 64
PITCH_PAD = 4
CHUNKS = 4
MESH = pl.DeviceIdType.MESH


def matmul_nt(left, right):
    return lax.dot_general(
        left, right, (((1,), (1,)), ((), ())), preferred_element_type=jnp.float32
    )


def split_terms(value):
    upper = value.astype(jnp.bfloat16)
    lower = (value - upper.astype(jnp.float32)).astype(jnp.bfloat16)
    return upper, lower


def chunk_count(ep_size):
    return CHUNKS if ep_size % CHUNKS == 0 else 1


def kernel(
    ep_size,
    tp_size,
    features_hbm,
    key_hbm,
    value_hbm,
    chosen_hbm,
    scores_hbm,
    out_ref,
    features,
    chosen,
    scores,
    picks,
    gates,
    key,
    key_columns,
    value,
    dense,
    partial,
    weights,
    summed,
    landed,
    local_sem,
    send_sem,
    recv_sem,
    tp_send,
    tp_recv,
    out_send,
    out_recv,
):
    my_ep = lax.axis_index("ep")
    my_tp = lax.axis_index("tp")
    table_rows = key.shape[0]
    blocks = table_rows // LANES
    own_tokens, heads, top = chosen_hbm.shape
    tokens = ep_size * own_tokens
    own_pairs = own_tokens // 2
    chunks = chunk_count(ep_size)
    chunk_owners = ep_size // chunks
    chunk_pairs = chunk_owners * own_pairs
    pitch = tokens + PITCH_PAD
    per_token = heads * top
    width = 2 * per_token

    def token_slot(ref, index):
        return ref.at[pl.ds(index * own_tokens, own_tokens)]

    def pair_slot(ref, index):
        return ref.at[pl.ds(pl.multiple_of(index * own_pairs, own_pairs), own_pairs)]

    small = (
        (features_hbm, token_slot(features, my_ep)),
        (chosen_hbm, chosen),
        (scores_hbm, scores),
    )
    small_copies = []
    for number, (source, target) in enumerate(small):
        copy = pltpu.make_async_copy(source, target, local_sem.at[number])
        copy.start()
        small_copies.append(copy)
    key_copy = pltpu.make_async_copy(key_hbm, key, local_sem.at[3])
    key_copy.start()
    value_copy = pltpu.make_async_copy(value_hbm, value, local_sem.at[4])
    value_copy.start()

    barrier = pltpu.get_barrier_semaphore()
    for step in range(1, ep_size):
        pl.semaphore_signal(
            barrier, inc=1, device_id=(lax.rem(my_ep + step, ep_size), my_tp), device_id_type=MESH
        )
    for step in range(1, tp_size):
        pl.semaphore_signal(
            barrier, inc=1, device_id=(my_ep, lax.rem(my_tp + step, tp_size)), device_id_type=MESH
        )
    for copy in small_copies:
        copy.wait()

    def packed(pieces):
        flat = jnp.concatenate(pieces, axis=1)
        return jnp.concatenate([flat[:own_pairs], flat[own_pairs:]], axis=1)

    pair_slot(picks, my_ep)[...] = packed([chosen[:, head, :] for head in range(heads)])
    gate_pieces = []
    for head in range(heads):
        logits = scores[:, head, :]
        powers = jnp.exp(logits - jnp.max(logits, axis=1, keepdims=True))
        gate_pieces.append(powers / jnp.sum(powers, axis=1, keepdims=True))
    pair_slot(gates, my_ep)[...] = packed(gate_pieces)
    pl.semaphore_wait(barrier, ep_size + tp_size - 2)

    def ep_copy(number, step, owner):
        slot = (
            token_slot(features, owner),
            pair_slot(picks, owner),
            pair_slot(gates, owner),
        )[number]
        return pltpu.make_async_remote_copy(
            src_ref=slot,
            dst_ref=slot,
            send_sem=send_sem.at[number, step - 1],
            recv_sem=recv_sem.at[number, step - 1],
            device_id=(lax.rem(my_ep + step, ep_size), my_tp),
            device_id_type=MESH,
        )

    def source_ep(step):
        return lax.rem(my_ep + ep_size - step, ep_size)

    for number in range(3):
        for step in range(1, ep_size):
            ep_copy(number, step, my_ep).start()

    depth = key.shape[1]

    def turn_step(index, carry):
        for inner in range(GROUP):
            block = index * GROUP + inner
            rows = key[pl.ds(pl.multiple_of(block * LANES, LANES), LANES), :]
            key_columns[pl.ds(pl.multiple_of(block * depth, depth), depth), :] = rows.T
        return carry

    key_copy.wait()
    lax.fori_loop(0, blocks // GROUP, turn_step, 0)

    for step in range(1, ep_size):
        ep_copy(0, step, source_ep(step)).wait_recv()
    token_vectors = features[...]

    def dense_step(index, carry):
        for inner in range(GROUP):
            block = index * GROUP + inner
            columns = key_columns[pl.ds(pl.multiple_of(block * depth, depth), depth), :]
            dense[pl.ds(block * pitch, tokens), :] = jnp.dot(
                token_vectors, columns, preferred_element_type=jnp.float32
            )
        return carry

    lax.fori_loop(0, blocks // GROUP, dense_step, 0)

    for step in range(1, ep_size):
        ep_copy(1, step, source_ep(step)).wait_recv()

    first_row = my_ep * table_rows
    block_ids = lax.broadcasted_iota(jnp.int32, (blocks, width), 0)
    lane_ids = lax.broadcasted_iota(jnp.int32, (LANES, width), 0)
    in_first = lax.broadcasted_iota(jnp.int32, (blocks, width), 1) < per_token

    def masks(pair):
        row = picks[pl.ds(pair, 1), :] - first_row
        column_hot = jnp.where((row & (LANES - 1)) == lane_ids, 1.0, 0.0).astype(jnp.bfloat16)
        block_mask = lax.shift_right_arithmetic(row, 7) == block_ids
        return column_hot, block_mask

    def chosen_of(token, column_hot):
        upper, lower = split_terms(dense[pl.ds(token, blocks, stride=pitch), :])
        return jnp.dot(upper, column_hot, preferred_element_type=jnp.float32) + jnp.dot(
            lower, column_hot, preferred_element_type=jnp.float32
        )

    def chunk_rows(chunk):
        return pl.ds(pl.multiple_of(chunk * chunk_pairs, chunk_pairs), chunk_pairs)

    def tp_copy(step, owner, chunk):
        slot = partial.at[owner, chunk_rows(chunk)]
        return pltpu.make_async_remote_copy(
            src_ref=slot,
            dst_ref=slot,
            send_sem=tp_send.at[step - 1, chunk],
            recv_sem=tp_recv.at[step - 1, chunk],
            device_id=(my_ep, lax.rem(my_tp + step, tp_size)),
            device_id_type=MESH,
        )

    def pick_step(owner, carry):
        for inner in range(own_pairs):
            pair = owner * own_pairs + inner
            token = owner * own_tokens + inner
            column_hot, block_mask = masks(pair)
            both = jnp.where(
                in_first,
                chosen_of(token, column_hot),
                chosen_of(token + own_pairs, column_hot),
            )
            partial[my_tp, pl.ds(pair, 1), :] = jnp.sum(
                jnp.where(block_mask, both, 0.0), axis=0, keepdims=True
            )
        return carry

    def pick_chunk(chunk, carry):
        if chunk_owners == 1:
            pick_step(chunk, 0)
        else:
            first = chunk * chunk_owners
            lax.fori_loop(first, first + chunk_owners, pick_step, 0)
        for step in range(1, tp_size):
            tp_copy(step, my_tp, chunk).start()
        return carry

    lax.fori_loop(0, chunks, pick_chunk, 0)

    for step in range(1, ep_size):
        ep_copy(2, step, source_ep(step)).wait_recv()
    def spread_step(owner, carry):
        for inner in range(own_pairs):
            pair = owner * own_pairs + inner
            first = owner * own_tokens + inner
            column_hot, block_mask = masks(pair)
            hot = jnp.where(block_mask, weights[pl.ds(pair, 1), :], 0.0)
            for token, keep in (
                (first, in_first),
                (first + own_pairs, jnp.logical_not(in_first)),
            ):
                dense[pl.ds(token, blocks, stride=pitch), :] = matmul_nt(
                    jnp.where(keep, hot, 0.0).astype(jnp.bfloat16), column_hot
                )
        return carry

    def spread_chunk(chunk, carry):
        for step in range(1, tp_size):
            tp_copy(step, lax.rem(my_tp + tp_size - step, tp_size), chunk).wait_recv()
        rows = chunk_rows(chunk)
        products = partial[0, rows, :]
        for index in range(1, tp_size):
            products = products + partial[index, rows, :]
        activated = 0.5 * products * (1.0 + lax.erf(products * (0.5**0.5)))
        row_weights = (gates[rows, :] * activated).astype(jnp.bfloat16)
        weights[rows, :] = row_weights.astype(jnp.float32)
        if chunk_owners == 1:
            spread_step(chunk, 0)
        else:
            first = chunk * chunk_owners
            lax.fori_loop(first, first + chunk_owners, spread_step, 0)
        return carry

    lax.fori_loop(0, chunks, spread_chunk, 0)

    value_copy.wait()

    def value_step(index, total):
        for inner in range(GROUP):
            block = index * GROUP + inner
            rows = value[pl.ds(pl.multiple_of(block * LANES, LANES), LANES), :]
            upper, lower = split_terms(
                dense[pl.ds(block * pitch, tokens), :]
            )
            both = jnp.concatenate([upper, lower], axis=0)
            total = total + jnp.dot(both, rows, preferred_element_type=jnp.float32)
        return total

    zero = jnp.zeros((2 * tokens, summed.shape[1]), jnp.float32)
    total = lax.fori_loop(0, blocks // GROUP, value_step, zero)
    summed[...] = total[:tokens] + total[tokens:]

    def out_copy(step, owner):
        return pltpu.make_async_remote_copy(
            src_ref=token_slot(summed, lax.rem(my_ep + step, ep_size)),
            dst_ref=landed.at[step - 1],
            send_sem=out_send.at[step - 1],
            recv_sem=out_recv.at[step - 1],
            device_id=(lax.rem(my_ep + step, ep_size), my_tp),
            device_id_type=MESH,
        )

    for step in range(1, ep_size):
        out_copy(step, my_ep).start()
    result = summed[pl.ds(pl.multiple_of(my_ep * own_tokens, own_tokens), own_tokens), :]
    for step in range(1, ep_size):
        out_copy(step, my_ep).wait_recv()
        result = result + landed[step - 1]
    out_ref[...] = result.astype(out_ref.dtype)

    for step in range(1, ep_size):
        for number in range(3):
            ep_copy(number, step, my_ep).wait_send()
        out_copy(step, my_ep).wait_send()
    for step in range(1, tp_size):
        for chunk in range(chunks):
            tp_copy(step, my_tp, chunk).wait_send()


def shards(ep_size, tp_size, features, key_table, value_table, chosen, scores):
    own_tokens, width = features.shape
    _, heads, top = chosen.shape
    table_rows = key_table.shape[0]
    tokens = ep_size * own_tokens
    packed_shape = (tokens // 2, 2 * heads * top)
    dma = pltpu.SemaphoreType.DMA
    return pl.pallas_call(
        functools.partial(kernel, ep_size, tp_size),
        out_shape=pltpu.VMEM((own_tokens, width), jnp.bfloat16),
        in_specs=[pl.BlockSpec(memory_space=pl.ANY)] * 5,
        out_specs=pl.BlockSpec(memory_space=pltpu.VMEM),
        scratch_shapes=[
            pltpu.VMEM((tokens, width), features.dtype),
            pltpu.VMEM((own_tokens, heads, top), jnp.int32),
            pltpu.VMEM((own_tokens, heads, top), jnp.float32),
            pltpu.VMEM(packed_shape, jnp.int32),
            pltpu.VMEM(packed_shape, jnp.float32),
            pltpu.VMEM((table_rows, width), key_table.dtype),
            pltpu.VMEM((table_rows // LANES * width, LANES), key_table.dtype),
            pltpu.VMEM((table_rows, width), value_table.dtype),
            pltpu.VMEM((table_rows // LANES * (tokens + PITCH_PAD), LANES), jnp.float32),
            pltpu.VMEM((tp_size,) + packed_shape, jnp.float32),
            pltpu.VMEM(packed_shape, jnp.float32),
            pltpu.VMEM((tokens, width), jnp.float32),
            pltpu.VMEM((ep_size - 1, own_tokens, width), jnp.float32),
            dma((5,)),
            dma((3, ep_size - 1)),
            dma((3, ep_size - 1)),
            dma((tp_size - 1, chunk_count(ep_size))),
            dma((tp_size - 1, chunk_count(ep_size))),
            dma((ep_size - 1,)),
            dma((ep_size - 1,)),
        ],
        compiler_params=pltpu.CompilerParams(collective_id=0, has_side_effects=True),
    )(features, key_table, value_table, chosen, scores)


def solution(mesh):
    return jax.shard_map(
        functools.partial(shards, mesh.shape["ep"], mesh.shape["tp"]),
        mesh=mesh,
        in_specs=(
            P("ep", "tp"),
            P("ep", "tp"),
            P("ep", "tp"),
            P("ep", None, None),
            P("ep", None, None),
        ),
        out_specs=P("ep", "tp"),
        check_vma=False,
    )
```

profile of v0, /device:TPU:1, one launch (start us, length us, event | category | flops | bytes accessed | tf_op | source)
XLA Modules:
  0.0 142.9 jit_solution(467414773918802953)
XLA Ops:
  0.0 0.0 copy-start
  0.0 4.7 %copy.6.key_hbm = bf16[16384,32]{1,0:T(8,128)(2,1)} copy(bf16[16384,32]{0,1:T(8,128)(2,1)} %param.6) | data formatting | bytes 2097152 | tf_op args[1]
  4.7 0.0 copy-done
  4.7 3.1 %copy.7.value_hbm = bf16[16384,32]{1,0:T(8,128)(2,1)} copy(bf16[16384,32]{0,1:T(8,128)(2,1)S(1)} %copy-done) | data formatting | bytes 2097152 | tf_op args[2]
  7.8 134.5 %shard_map.55 = bf16[16,32]{1,0:T(8,128)(2,1)S(1)} custom-call(bf16[16,32]{1,0:T(8,128)(2,1)} %features_hbm.1, bf16[16384,32]{1,0:T(8,128)(2,1)} %copy.6.key_hbm, bf16[16384,32]{1,0:T(8,128)(2,1)} %copy.7.value_hbm, s32[16,4,16]{2,1,0:T(4,128)} %chosen_hbm.1, f32[16,4,16]{2,1,0:T(4,128)} %scores_hbm.1), custom_call_target="tpu_custom_call" | custom-call | tf_op jit(solution)/shard_map/pallas_call | solution.py:320
  142.3 0.6 copy.9
Async XLA Ops:
  0.0 4.7 %copy-start = (bf16[16384,32]{0,1:T(8,128)(2,1)S(1)}, bf16[16384,32]{0,1:T(8,128)(2,1)}, u32[]{:S(2)}) copy-start(bf16[16384,32]{0,1:T(8,128)(2,1)} %param.7) | copy-start | bytes 3145732
where the time goes:
time: 143 us
  Pallas kernels  135 us (94%)
  local copies, waits for them, and re-layouts  8.38 us (6%)
    pallas_call x1, Pallas kernels, shards(): pl.pallas_call(functools.partial(kernel, ep_size, tp_size), out_shape=plt...  135 us
    unnamed x5, local copies, waits for them, and re-layouts  8.38 us

commit v1 on v0

v1 whole, which is shorter than its diff:
```python
import functools

import jax
import jax.numpy as jnp
from jax import lax
from jax.experimental import pallas as pl
from jax.experimental.pallas import tpu as pltpu
from jax.sharding import PartitionSpec as P

LANES = 128
CORES = 2
PITCH_PAD = 4
GROUP = 4
UNROLL = 16
MESH = pl.DeviceIdType.MESH


def matmul_nt(left, right):
    return lax.dot_general(
        left, right, (((1,), (1,)), ((), ())), preferred_element_type=jnp.float32
    )


def kernel(
    ep_size,
    z_size,
    features_hbm,
    key_hbm,
    value_hbm,
    chosen_hbm,
    scores_hbm,
    out_ref,
    feature_parts,
    features,
    chosen,
    scores,
    picks,
    gates,
    key,
    value,
    dense_even,
    dense_odd,
    partial,
    landed,
    weights,
    spread,
    summed,
    out_landed,
    local_sem,
    table_send,
    table_recv,
    feature_send,
    feature_recv,
    pick_send,
    pick_recv,
    gate_send,
    gate_recv,
    part_send,
    part_recv,
    weight_send,
    weight_recv,
    out_send,
    out_recv,
):
    my_ep = lax.axis_index("ep")
    my_tp = lax.axis_index("tp")
    my_z = my_tp // CORES
    my_core = my_tp % CORES
    other_core = 1 - my_core
    partner = my_z * CORES + other_core
    width = features_hbm.shape[1]
    own_tokens, heads, top = chosen_hbm.shape
    per_token = heads * top
    own_pairs = own_tokens // 2
    half_rows = key.shape[1]
    blocks = half_rows // LANES
    chunk_tokens = GROUP * own_tokens
    pitch = chunk_tokens + PITCH_PAD
    chunks = ep_size // GROUP

    def ep_at(step):
        return lax.rem(my_ep + step, ep_size)

    def z_at(step):
        return lax.rem(my_z + step, z_size)

    def tokens_of(index):
        return pl.ds(pl.multiple_of(index * own_tokens, own_tokens), own_tokens)

    def pairs_of(index):
        return pl.ds(pl.multiple_of(index * own_pairs, own_pairs), own_pairs)

    own_features = feature_parts.at[my_core, tokens_of(my_ep)]
    small = (
        (features_hbm, own_features),
        (chosen_hbm, chosen),
        (scores_hbm, scores),
    )
    small_copies = []
    for number, (source, target) in enumerate(small):
        copy = pltpu.make_async_copy(source, target, local_sem.at[number])
        copy.start()
        small_copies.append(copy)
    half_of = pl.ds(pl.multiple_of(my_core * half_rows, half_rows), half_rows)
    other_half = pl.ds(pl.multiple_of(other_core * half_rows, half_rows), half_rows)
    my_width = pl.ds(pl.multiple_of(my_core * width, width), width)
    table_copies = []
    for number, (source, target) in enumerate(((key_hbm, key), (value_hbm, value))):
        copy = pltpu.make_async_copy(
            source.at[:, half_of], target.at[my_width, :], local_sem.at[3 + number]
        )
        copy.start()
        table_copies.append(copy)

    barrier = pltpu.get_barrier_semaphore()

    def greet(ep, tp):
        pl.semaphore_signal(barrier, inc=1, device_id=(ep, tp), device_id_type=MESH)

    for step in range(1, z_size):
        greet(my_ep, z_at(step) * CORES + my_core)
    for step in range(1, ep_size):
        greet(ep_at(step), my_tp)
        greet(ep_at(step), partner)
    greet(my_ep, partner)

    for copy in small_copies:
        copy.wait()

    def packed(pieces):
        flat = jnp.concatenate(pieces, axis=1)
        return jnp.concatenate([flat[:own_pairs], flat[own_pairs:]], axis=1)

    picks[pairs_of(my_ep), :] = packed([chosen[:, head, :] for head in range(heads)])
    gate_pieces = []
    for head in range(heads):
        logits = scores[:, head, :]
        powers = jnp.exp(logits - jnp.max(logits, axis=1, keepdims=True))
        gate_pieces.append(powers / jnp.sum(powers, axis=1, keepdims=True))

    @pl.when(my_ep == my_z)
    def _():
        gates[...] = packed(gate_pieces)

    pl.semaphore_wait(barrier, z_size - 1 + CORES * (ep_size - 1) + 1)

    def remote(source, target, send, recv, ep, tp):
        return pltpu.make_async_remote_copy(
            src_ref=source,
            dst_ref=target,
            send_sem=send,
            recv_sem=recv,
            device_id=(ep, tp),
            device_id_type=MESH,
        )

    def pick_copy(step, owner):
        slot = picks.at[pairs_of(owner)]
        return remote(
            slot, slot, pick_send.at[step - 1], pick_recv.at[step - 1], ep_at(step), my_tp
        )

    def feature_copy(step, owner, source_core, cross):
        slot = feature_parts.at[source_core, tokens_of(owner)]
        return remote(
            slot,
            slot,
            feature_send.at[cross, step],
            feature_recv.at[cross, step],
            ep_at(step),
            partner if cross else my_tp,
        )

    def gate_copy(step):
        return remote(
            gates, gates, gate_send.at[step - 1], gate_recv.at[0], ep_at(step), my_tp
        )

    def table_copy(number):
        source, target = ((key_hbm, key), (value_hbm, value))[number]
        return remote(
            source.at[:, other_half],
            target.at[my_width, :],
            table_send.at[number],
            table_recv.at[number],
            my_ep,
            partner,
        )

    for step in range(1, ep_size):
        feature_copy(step, my_ep, my_core, 0).start()
        feature_copy(step, my_ep, my_core, 1).start()
        pick_copy(step, my_ep).start()
    feature_copy(0, my_ep, my_core, 1).start()
    table_copy(0).start()

    @pl.when(my_ep == my_z)
    def _():
        for step in range(1, ep_size):
            gate_copy(step).start()

    table_copy(1).start()

    def source_ep(step):
        return lax.rem(my_ep + ep_size - step, ep_size)

    for step in range(1, ep_size):
        feature_copy(step, source_ep(step), my_core, 0).wait_recv()
    for step in range(ep_size):
        feature_copy(step, source_ep(step), other_core, 1).wait_recv()
    features[...] = jnp.concatenate([feature_parts[0], feature_parts[1]], axis=1)
    for step in range(1, ep_size):
        pick_copy(step, source_ep(step)).wait_recv()
    table_copies[0].wait()

    def table_landed(number):
        target = (key, value)[number]
        other_width = pl.ds(pl.multiple_of(other_core * width, width), width)
        return remote(
            (key_hbm, value_hbm)[number].at[:, other_half],
            target.at[other_width, :],
            table_send.at[number],
            table_recv.at[number],
            my_ep,
            partner,
        )

    table_landed(0).wait_recv()

    first_row = (my_ep * CORES + my_core) * half_rows
    in_first = lax.broadcasted_iota(jnp.int32, (own_pairs, LANES), 1) < per_token

    def far_slice(place):
        half = (place + 1) // 2
        offset = z_size // 2 + jnp.where(place % 2 == 0, half, -half)
        return z_at(offset)

    def part_copy(step, target_z):
        return remote(
            partial.at[target_z],
            landed.at[step - 1],
            part_send.at[step - 1],
            part_recv.at[step - 1],
            my_ep,
            target_z * CORES + my_core,
        )

    steps = blocks // UNROLL

    def dense_step(group, step, target):
        rows = jnp.concatenate(
            [features[tokens_of(far_slice(group * GROUP + inner)), :] for inner in range(GROUP)],
            axis=0,
        )
        columns = key[:, step * UNROLL * LANES : (step + 1) * UNROLL * LANES]
        target[...] = jnp.dot(rows, columns, preferred_element_type=jnp.float32)

    def take_step(step, source, found, wanted):
        for inner in range(GROUP):
            row = wanted[inner]
            lane = row & (LANES - 1)
            block = lax.shift_right_arithmetic(row, 7)
            first = inner * own_tokens
            for offset in range(UNROLL):
                columns = slice(offset * LANES, (offset + 1) * LANES)
                upper = jnp.take_along_axis(
                    source[first : first + own_pairs, columns], lane, axis=1
                )
                lower = jnp.take_along_axis(
                    source[first + own_pairs : first + own_tokens, columns], lane, axis=1
                )
                found[inner] = jnp.where(
                    block == step * UNROLL + offset,
                    jnp.where(in_first, upper, lower),
                    found[inner],
                )

    dense_step(0, 0, dense_even)

    def pick_group(group, carry):
        slices = [far_slice(group * GROUP + inner) for inner in range(GROUP)]
        wanted = [picks[pairs_of(index), :] - first_row for index in slices]
        found = [jnp.zeros((own_pairs, LANES), jnp.float32)] * GROUP
        buffers = (dense_even, dense_odd)
        for step in range(steps):
            if step + 1 < steps:
                dense_step(group, step + 1, buffers[(step + 1) % 2])
            else:
                dense_step(jnp.minimum(group + 1, chunks - 1), 0, buffers[(step + 1) % 2])
            take_step(step, buffers[step % 2], found, wanted)
        for inner in range(GROUP):
            partial[slices[inner]] = found[inner]
        for inner in range(GROUP):
            index = slices[inner]
            step = lax.rem(index - my_z + z_size, z_size)

            @pl.when(step != 0)
            def _():
                part_copy(step, index).start()

        return carry

    lax.fori_loop(0, chunks, pick_group, 0)

    @pl.when(my_ep != my_z)
    def _():
        gate_copy(1).wait_recv()

    products = partial[my_z]
    for step in range(1, z_size):
        part_copy(step, my_z).wait_recv()
        products = products + landed[step - 1]
    activated = 0.5 * products * (1.0 + lax.erf(products * (0.5**0.5)))
    weights[my_z] = (gates[...] * activated).astype(jnp.bfloat16).astype(jnp.float32)

    def weight_copy(step, owner):
        slot = weights.at[owner]
        return remote(
            slot,
            slot,
            weight_send.at[step - 1],
            weight_recv.at[step - 1],
            my_ep,
            z_at(step) * CORES + my_core,
        )

    for step in range(1, z_size):
        weight_copy(step, my_z).start()

    table_copies[1].wait()
    table_landed(1).wait_recv()

    def near_offset(place):
        half = (place + 1) // 2
        return jnp.where(place % 2 == 1, half, lax.rem(z_size - half, z_size))

    block_ids = lax.broadcasted_iota(jnp.int32, (blocks, LANES), 0)
    lane_ids = lax.broadcasted_iota(jnp.int32, (LANES, LANES), 0)
    block_first = lax.broadcasted_iota(jnp.int32, (blocks, LANES), 1) < per_token

    def out_copy(token_block, target_core, cross, target_z_slot):
        step = lax.rem(token_block - my_ep + ep_size, ep_size)
        return remote(
            summed.at[target_core, tokens_of(target_z_slot)],
            out_landed.at[cross, step],
            out_send.at[cross, step],
            out_recv.at[cross, step],
            token_block,
            my_z * CORES + target_core,
        )

    def spread_chunk(chunk, carry):
        def spread_slice(inner, inner_carry):
            offset = near_offset(chunk * GROUP + inner)
            index = z_at(offset)

            @pl.when(offset != 0)
            def _():
                weight_copy(z_size - offset, index).wait_recv()

            for row_index in range(own_pairs):
                row = picks[pl.ds(index * own_pairs + row_index, 1), :] - first_row
                weight = weights[index, row_index : row_index + 1, :]
                column_hot = jnp.where(
                    (row & (LANES - 1)) == lane_ids, 1.0, 0.0
                ).astype(jnp.bfloat16)
                block_mask = lax.shift_right_arithmetic(row, 7) == block_ids
                hot = jnp.where(block_mask, weight, 0.0)
                both = jnp.concatenate(
                    [
                        jnp.where(block_first, hot, 0.0).astype(jnp.bfloat16),
                        jnp.where(block_first, 0.0, hot).astype(jnp.bfloat16),
                    ],
                    axis=0,
                )
                placed = matmul_nt(both, column_hot)
                token = inner * own_tokens + row_index
                spread[pl.ds(token, blocks, stride=pitch), :] = placed[:blocks]
                spread[pl.ds(token + own_pairs, blocks, stride=pitch), :] = placed[blocks:]
            return inner_carry

        lax.fori_loop(0, GROUP, spread_slice, 0)
        rows = jnp.concatenate(
            [
                spread[block * pitch : block * pitch + chunk_tokens, :].astype(jnp.bfloat16)
                for block in range(blocks)
            ],
            axis=1,
        )
        total = matmul_nt(rows, value[...])
        for inner in range(GROUP):
            index = z_at(near_offset(chunk * GROUP + inner))
            piece = total[inner * own_tokens : (inner + 1) * own_tokens]
            for target_core in range(CORES):
                summed[target_core, tokens_of(index), :] = piece[
                    :, target_core * width : (target_core + 1) * width
                ]
        for inner in range(GROUP):
            index = z_at(near_offset(chunk * GROUP + inner))

            @pl.when(index != my_ep)
            def _():
                out_copy(index, my_core, 0, index).start()

            out_copy(index, other_core, 1, index).start()
        return carry

    lax.fori_loop(0, chunks, spread_chunk, 0)

    result = summed[my_core, tokens_of(my_ep), :]
    for cross in range(CORES):
        for step in range(1 - cross, ep_size):
            remote(
                summed.at[0, tokens_of(0)],
                out_landed.at[cross, step],
                out_send.at[cross, step],
                out_recv.at[cross, step],
                ep_at(step),
                my_tp,
            ).wait_recv()
            result = result + out_landed[cross, step]
    out_ref[...] = result.astype(out_ref.dtype)

    for step in range(1, ep_size):
        feature_copy(step, my_ep, my_core, 0).wait_send()
        feature_copy(step, my_ep, my_core, 1).wait_send()
        pick_copy(step, my_ep).wait_send()
    feature_copy(0, my_ep, my_core, 1).wait_send()

    @pl.when(my_ep == my_z)
    def _():
        for step in range(1, ep_size):
            gate_copy(step).wait_send()

    for number in range(2):
        table_copy(number).wait_send()
    for step in range(1, z_size):
        part_copy(step, z_at(step)).wait_send()
        weight_copy(step, my_z).wait_send()
    for cross in range(CORES):
        for step in range(1 - cross, ep_size):
            out_copy(
                ep_at(step), other_core if cross else my_core, cross, ep_at(step)
            ).wait_send()


def shards(ep_size, tp_size, features, key_table, value_table, chosen, scores):
    own_tokens, width = features.shape
    _, heads, top = chosen.shape
    half_rows = key_table.shape[0] // CORES
    z_size = tp_size // CORES
    tokens = ep_size * own_tokens
    own_pairs = own_tokens // 2
    blocks = half_rows // LANES
    chunk_tokens = GROUP * own_tokens
    dma = pltpu.SemaphoreType.DMA
    slices = (z_size, own_pairs, LANES)
    return pl.pallas_call(
        functools.partial(kernel, ep_size, z_size),
        out_shape=pltpu.VMEM((own_tokens, width), jnp.bfloat16),
        in_specs=[pl.BlockSpec(memory_space=pl.ANY)] * 5,
        out_specs=pl.BlockSpec(memory_space=pltpu.VMEM),
        scratch_shapes=[
            pltpu.VMEM((CORES, tokens, width), features.dtype),
            pltpu.VMEM((tokens, CORES * width), features.dtype),
            pltpu.VMEM((own_tokens, heads, top), jnp.int32),
            pltpu.VMEM((own_tokens, heads, top), jnp.float32),
            pltpu.VMEM((tokens // 2, LANES), jnp.int32),
            pltpu.VMEM((own_pairs, LANES), jnp.float32),
            pltpu.VMEM((CORES * width, half_rows), key_table.dtype),
            pltpu.VMEM((CORES * width, half_rows), value_table.dtype),
            pltpu.VMEM((chunk_tokens, UNROLL * LANES), jnp.float32),
            pltpu.VMEM((chunk_tokens, UNROLL * LANES), jnp.float32),
            pltpu.VMEM(slices, jnp.float32),
            pltpu.VMEM((z_size - 1,) + slices[1:], jnp.float32),
            pltpu.VMEM(slices, jnp.float32),
            pltpu.VMEM((blocks * (chunk_tokens + PITCH_PAD), LANES), jnp.float32),
            pltpu.VMEM((CORES, tokens, width), jnp.float32),
            pltpu.VMEM((CORES, ep_size, own_tokens, width), jnp.float32),
            dma((5,)),
            dma((2,)),
            dma((2,)),
            dma((CORES, ep_size)),
            dma((CORES, ep_size)),
            dma((ep_size - 1,)),
            dma((ep_size - 1,)),
            dma((ep_size - 1,)),
            dma((1,)),
            dma((z_size - 1,)),
            dma((z_size - 1,)),
            dma((z_size - 1,)),
            dma((z_size - 1,)),
            dma((CORES, ep_size)),
            dma((CORES, ep_size)),
        ],
        compiler_params=pltpu.CompilerParams(collective_id=0, has_side_effects=True),
    )(features, key_table.T, value_table.T, chosen, scores)


def solution(mesh):
    return jax.shard_map(
        functools.partial(shards, mesh.shape["ep"], mesh.shape["tp"]),
        mesh=mesh,
        in_specs=(
            P("ep", "tp"),
            P("ep", "tp"),
            P("ep", "tp"),
            P("ep", None, None),
            P("ep", None, None),
        ),
        out_specs=P("ep", "tp"),
        check_vma=False,
    )
```

time: 143 us -> 46.8 us (0.33)
  the two profiles are of different devices: /device:TPU:1 before, /device:TPU:17 now
where the time goes in v1:
time: 46.8 us; the launch traced here: 46.7 us
  Pallas kernels  46.1 us (99%)
  local copies, waits for them, and re-layouts  0.6 us (1%)
    pallas_call x1, Pallas kernels, shards(): pl.pallas_call(functools.partial(kernel, ep_size, z_size), out_shape=pltp...  46.1 us

profile of v1, /device:TPU:17, one launch (start us, length us, event | category | flops | bytes accessed | tf_op | source)
XLA Modules:
  0.0 46.7 jit_solution(9472268029676138897)
XLA Ops:
  0.0 46.1 %shard_map.55 = bf16[16,32]{1,0:T(8,128)(2,1)S(1)} custom-call(bf16[16,32]{1,0:T(8,128)(2,1)} %features_hbm.1, bf16[32,16384]{1,0:T(8,128)(2,1)} %bitcast.2, bf16[32,16384]{1,0:T(8,128)(2,1)} %bitcast.3, s32[16,4,16]{2,1,0:T(4,128)} %chosen_hbm.1, f32[16,4,16]{2,1,0:T(4,128)} %scores_hbm.1), custom_call_target="tpu_custom_call" | custom-call | tf_op jit(solution)/shard_map/pallas_call | solution.py:458
  46.1 0.6 %copy.7 = bf16[16,32]{1,0:T(8,128)(2,1)} copy(bf16[16,32]{1,0:T(8,128)(2,1)S(1)} %shard_map.55) | data formatting | bytes 2048

commit v2 on v1

--- a/solution.py
+++ b/solution.py
@@ -46,6 +46,7 @@
     spread,
     summed,
     out_landed,
+    far_sem,
     local_sem,
     table_send,
     table_recv,
@@ -113,12 +114,14 @@
         table_copies.append(copy)
 
     barrier = pltpu.get_barrier_semaphore()
+    reach = z_size // 4
 
     def greet(ep, tp):
         pl.semaphore_signal(barrier, inc=1, device_id=(ep, tp), device_id_type=MESH)
 
     for step in range(1, z_size):
-        greet(my_ep, z_at(step) * CORES + my_core)
+        if min(step, z_size - step) <= reach:
+            greet(my_ep, z_at(step) * CORES + my_core)
     for step in range(1, ep_size):
         greet(ep_at(step), my_tp)
         greet(ep_at(step), partner)
@@ -142,7 +145,14 @@
     def _():
         gates[...] = packed(gate_pieces)
 
-    pl.semaphore_wait(barrier, z_size - 1 + CORES * (ep_size - 1) + 1)
+    pl.semaphore_wait(barrier, 2 * reach + CORES * (ep_size - 1) + 1)
+    for step in (reach, z_size - reach):
+        pl.semaphore_signal(
+            far_sem,
+            inc=1,
+            device_id=(my_ep, z_at(step) * CORES + my_core),
+            device_id_type=MESH,
+        )
 
     def remote(source, target, send, recv, ep, tp):
         return pltpu.make_async_remote_copy(
@@ -198,8 +208,6 @@
     def _():
         for step in range(1, ep_size):
             gate_copy(step).start()
-
-    table_copy(1).start()
 
     def source_ep(step):
         return lax.rem(my_ep + ep_size - step, ep_size)
@@ -276,6 +284,7 @@
                 )
 
     dense_step(0, 0, dense_even)
+    pl.semaphore_wait(far_sem, 2)
 
     def pick_group(group, carry):
         slices = [far_slice(group * GROUP + inner) for inner in range(GROUP)]
@@ -301,6 +310,7 @@
         return carry
 
     lax.fori_loop(0, chunks, pick_group, 0)
+    table_copy(1).start()
 
     @pl.when(my_ep != my_z)
     def _():
@@ -311,7 +321,7 @@
         part_copy(step, my_z).wait_recv()
         products = products + landed[step - 1]
     activated = 0.5 * products * (1.0 + lax.erf(products * (0.5**0.5)))
-    weights[my_z] = (gates[...] * activated).astype(jnp.bfloat16).astype(jnp.float32)
+    weights[my_z] = (gates[...] * activated).astype(jnp.bfloat16)
 
     def weight_copy(step, owner):
         slot = weights.at[owner]
@@ -358,9 +368,10 @@
             def _():
                 weight_copy(z_size - offset, index).wait_recv()
 
+            slice_weights = weights[index].astype(jnp.float32)
             for row_index in range(own_pairs):
                 row = picks[pl.ds(index * own_pairs + row_index, 1), :] - first_row
-                weight = weights[index, row_index : row_index + 1, :]
+                weight = slice_weights[row_index : row_index + 1]
                 column_hot = jnp.where(
                     (row & (LANES - 1)) == lane_ids, 1.0, 0.0
                 ).astype(jnp.bfloat16)
@@ -473,10 +484,11 @@
             pltpu.VMEM((chunk_tokens, UNROLL * LANES), jnp.float32),
             pltpu.VMEM(slices, jnp.float32),
             pltpu.VMEM((z_size - 1,) + slices[1:], jnp.float32),
-            pltpu.VMEM(slices, jnp.float32),
+            pltpu.VMEM(slices, jnp.bfloat16),
             pltpu.VMEM((blocks * (chunk_tokens + PITCH_PAD), LANES), jnp.float32),
             pltpu.VMEM((CORES, tokens, width), jnp.float32),
             pltpu.VMEM((CORES, ep_size, own_tokens, width), jnp.float32),
+            pltpu.SemaphoreType.REGULAR,
             dma((5,)),
             dma((2,)),
             dma((2,)),

time: 46.8 us -> 45 us (0.962)
  Pallas kernels: 46.1 us -> 44.3 us
    pallas_call x1, Pallas kernels: 46.1 us -> 44.3 us  [shards(): pl.pallas_call(functools.partial(kernel, ep_size, z_size), out_shape=pltp...]
where the time goes in v2:
time: 45 us; the launch traced here: 44.9 us
  Pallas kernels  44.3 us (98%)
  local copies, waits for them, and re-layouts  0.6 us (1%)
    pallas_call x1, Pallas kernels, shards(): pl.pallas_call(functools.partial(kernel, ep_size, z_size), out_shape=pltp...  44.3 us

profile of v2, /device:TPU:17, one launch (start us, length us, event | category | flops | bytes accessed | tf_op | source)
XLA Modules:
  0.0 44.9 jit_solution(3213485589576234654)
XLA Ops:
  0.0 44.3 %shard_map.55 = bf16[16,32]{1,0:T(8,128)(2,1)S(1)} custom-call(bf16[16,32]{1,0:T(8,128)(2,1)} %features_hbm.1, bf16[32,16384]{1,0:T(8,128)(2,1)} %bitcast.2, bf16[32,16384]{1,0:T(8,128)(2,1)} %bitcast.3, s32[16,4,16]{2,1,0:T(4,128)} %chosen_hbm.1, f32[16,4,16]{2,1,0:T(4,128)} %scores_hbm.1), custom_call_target="tpu_custom_call" | custom-call | tf_op jit(solution)/shard_map/pallas_call | solution.py:469
  44.3 0.6 %copy.7 = bf16[16,32]{1,0:T(8,128)(2,1)} copy(bf16[16,32]{1,0:T(8,128)(2,1)S(1)} %shard_map.55) | data formatting | bytes 2048

commit v3 on v2

--- a/solution.py
+++ b/solution.py
@@ -1,4 +1,5 @@
 import functools
+import math
 
 import jax
 import jax.numpy as jnp
@@ -11,6 +12,7 @@
 CORES = 2
 PITCH_PAD = 4
 GROUP = 4
+LAST = 2
 UNROLL = 16
 MESH = pl.DeviceIdType.MESH
 
@@ -30,6 +32,7 @@
     chosen_hbm,
     scores_hbm,
     out_ref,
+    own_features,
     feature_parts,
     features,
     chosen,
@@ -75,12 +78,33 @@
     own_pairs = own_tokens // 2
     half_rows = key.shape[1]
     blocks = half_rows // LANES
-    chunk_tokens = GROUP * own_tokens
-    pitch = chunk_tokens + PITCH_PAD
     chunks = ep_size // GROUP
 
+    side = math.isqrt(ep_size)
+    folds = LANES // width
+    fold_rows = own_tokens // folds
+
     def ep_at(step):
-        return lax.rem(my_ep + step, ep_size)
+        down, across = step // side, step % side
+        return lax.rem(my_ep // side + down, side) * side + lax.rem(
+            my_ep + across, side
+        )
+
+    def source_ep(step):
+        down, across = step // side, step % side
+        return lax.rem(my_ep // side + side - down, side) * side + lax.rem(
+            my_ep + side - across, side
+        )
+
+    def hops(step):
+        down, across = step // side, step % side
+        return min(down, side - down) + min(across, side - across)
+
+    far_first = sorted(range(1, ep_size), key=hops, reverse=True)
+
+    def ep_step(target):
+        down = lax.rem(target // side - my_ep // side + side, side)
+        return down * side + lax.rem(target - my_ep + ep_size, side)
 
     def z_at(step):
         return lax.rem(my_z + step, z_size)
@@ -91,7 +115,6 @@
     def pairs_of(index):
         return pl.ds(pl.multiple_of(index * own_pairs, own_pairs), own_pairs)
 
-    own_features = feature_parts.at[my_core, tokens_of(my_ep)]
     small = (
         (features_hbm, own_features),
         (chosen_hbm, chosen),
@@ -119,16 +142,27 @@
     def greet(ep, tp):
         pl.semaphore_signal(barrier, inc=1, device_id=(ep, tp), device_id_type=MESH)
 
-    for step in range(1, z_size):
-        if min(step, z_size - step) <= reach:
-            greet(my_ep, z_at(step) * CORES + my_core)
-    for step in range(1, ep_size):
+    for step in far_first:
         greet(ep_at(step), my_tp)
         greet(ep_at(step), partner)
+        if step <= reach:
+            greet(my_ep, z_at(reach + 1 - step) * CORES + my_core)
+            greet(my_ep, z_at(z_size - reach - 1 + step) * CORES + my_core)
     greet(my_ep, partner)
 
     for copy in small_copies:
         copy.wait()
+
+    tokens_here = own_features[...].astype(jnp.float32)
+    feature_parts[my_core, my_ep] = jnp.concatenate(
+        [tokens_here[fold * fold_rows : (fold + 1) * fold_rows] for fold in range(folds)],
+        axis=1,
+    ).astype(jnp.bfloat16)
+
+    def unfolded(tile):
+        return jnp.concatenate(
+            [tile[:, fold * width : (fold + 1) * width] for fold in range(folds)], axis=0
+        )
 
     def packed(pieces):
         flat = jnp.concatenate(pieces, axis=1)
@@ -171,7 +205,7 @@
         )
 
     def feature_copy(step, owner, source_core, cross):
-        slot = feature_parts.at[source_core, tokens_of(owner)]
+        slot = feature_parts.at[source_core, owner]
         return remote(
             slot,
             slot,
@@ -197,7 +231,7 @@
             partner,
         )
 
-    for step in range(1, ep_size):
+    for step in far_first:
         feature_copy(step, my_ep, my_core, 0).start()
         feature_copy(step, my_ep, my_core, 1).start()
         pick_copy(step, my_ep).start()
@@ -206,17 +240,21 @@
 
     @pl.when(my_ep == my_z)
     def _():
-        for step in range(1, ep_size):
+        for step in far_first:
             gate_copy(step).start()
-
-    def source_ep(step):
-        return lax.rem(my_ep + ep_size - step, ep_size)
 
     for step in range(1, ep_size):
         feature_copy(step, source_ep(step), my_core, 0).wait_recv()
     for step in range(ep_size):
         feature_copy(step, source_ep(step), other_core, 1).wait_recv()
-    features[...] = jnp.concatenate([feature_parts[0], feature_parts[1]], axis=1)
+    for owner in range(ep_size):
+        features[owner * own_tokens : (owner + 1) * own_tokens, :] = jnp.concatenate(
+            [
+                unfolded(feature_parts[core, owner].astype(jnp.float32))
+                for core in range(CORES)
+            ],
+            axis=1,
+        ).astype(jnp.bfloat16)
     for step in range(1, ep_size):
         pick_copy(step, source_ep(step)).wait_recv()
     table_copies[0].wait()
@@ -348,20 +386,23 @@
     lane_ids = lax.broadcasted_iota(jnp.int32, (LANES, LANES), 0)
     block_first = lax.broadcasted_iota(jnp.int32, (blocks, LANES), 1) < per_token
 
-    def out_copy(token_block, target_core, cross, target_z_slot):
-        step = lax.rem(token_block - my_ep + ep_size, ep_size)
-        return remote(
-            summed.at[target_core, tokens_of(target_z_slot)],
+    def out_copy(step, target, cross):
+        target_core = other_core if cross else my_core
+        return remote(
+            summed.at[target_core, target],
             out_landed.at[cross, step],
             out_send.at[cross, step],
             out_recv.at[cross, step],
-            token_block,
+            target,
             my_z * CORES + target_core,
         )
 
-    def spread_chunk(chunk, carry):
-        def spread_slice(inner, inner_carry):
-            offset = near_offset(chunk * GROUP + inner)
+    def spread_chunk(first, size):
+        quarter = fold_rows * size
+        pitch = folds * quarter + PITCH_PAD
+
+        def spread_slice(inner, carry):
+            offset = near_offset(first + inner)
             index = z_at(offset)
 
             @pl.when(offset != 0)
@@ -369,9 +410,9 @@
                 weight_copy(z_size - offset, index).wait_recv()
 
             slice_weights = weights[index].astype(jnp.float32)
-            for row_index in range(own_pairs):
-                row = picks[pl.ds(index * own_pairs + row_index, 1), :] - first_row
-                weight = slice_weights[row_index : row_index + 1]
+            for pair in range(own_pairs):
+                row = picks[pl.ds(index * own_pairs + pair, 1), :] - first_row
+                weight = slice_weights[pair : pair + 1]
                 column_hot = jnp.where(
                     (row & (LANES - 1)) == lane_ids, 1.0, 0.0
                 ).astype(jnp.bfloat16)
@@ -385,52 +426,68 @@
                     axis=0,
                 )
                 placed = matmul_nt(both, column_hot)
-                token = inner * own_tokens + row_index
-                spread[pl.ds(token, blocks, stride=pitch), :] = placed[:blocks]
-                spread[pl.ds(token + own_pairs, blocks, stride=pitch), :] = placed[blocks:]
-            return inner_carry
-
-        lax.fori_loop(0, GROUP, spread_slice, 0)
+                for half in range(2):
+                    fold, row_in_fold = divmod(half * own_pairs + pair, fold_rows)
+                    place = fold * quarter + inner * fold_rows + row_in_fold
+                    spread[pl.ds(place, blocks, stride=pitch), :] = placed[
+                        half * blocks : (half + 1) * blocks
+                    ]
+            return carry
+
+        lax.fori_loop(0, size, spread_slice, 0)
         rows = jnp.concatenate(
             [
-                spread[block * pitch : block * pitch + chunk_tokens, :].astype(jnp.bfloat16)
+                spread[block * pitch : block * pitch + folds * quarter, :].astype(
+                    jnp.bfloat16
+                )
                 for block in range(blocks)
             ],
             axis=1,
         )
         total = matmul_nt(rows, value[...])
-        for inner in range(GROUP):
-            index = z_at(near_offset(chunk * GROUP + inner))
-            piece = total[inner * own_tokens : (inner + 1) * own_tokens]
-            for target_core in range(CORES):
-                summed[target_core, tokens_of(index), :] = piece[
-                    :, target_core * width : (target_core + 1) * width
+        targets = [z_at(near_offset(first + inner)) for inner in range(size)]
+        for core in range(CORES):
+            piece = jnp.concatenate(
+                [
+                    total[
+                        fold * quarter : (fold + 1) * quarter,
+                        core * width : (core + 1) * width,
+                    ]
+                    for fold in range(folds)
+                ],
+                axis=1,
+            )
+            for inner in range(size):
+                summed[core, targets[inner]] = piece[
+                    inner * fold_rows : (inner + 1) * fold_rows
                 ]
-        for inner in range(GROUP):
-            index = z_at(near_offset(chunk * GROUP + inner))
-
-            @pl.when(index != my_ep)
+        for inner in range(size):
+            target = targets[inner]
+            step = ep_step(target)
+
+            @pl.when(step != 0)
             def _():
-                out_copy(index, my_core, 0, index).start()
-
-            out_copy(index, other_core, 1, index).start()
+                out_copy(step, target, 0).start()
+
+            out_copy(step, target, 1).start()
+
+    def spread_large(chunk, carry):
+        spread_chunk(chunk * GROUP, GROUP)
         return carry
 
-    lax.fori_loop(0, chunks, spread_chunk, 0)
-
-    result = summed[my_core, tokens_of(my_ep), :]
+    def spread_small(chunk, carry):
+        spread_chunk(z_size - GROUP + chunk * LAST, LAST)
+        return carry
+
+    lax.fori_loop(0, chunks - 1, spread_large, 0)
+    lax.fori_loop(0, GROUP // LAST, spread_small, 0)
+
+    result = summed[my_core, my_ep]
     for cross in range(CORES):
         for step in range(1 - cross, ep_size):
-            remote(
-                summed.at[0, tokens_of(0)],
-                out_landed.at[cross, step],
-                out_send.at[cross, step],
-                out_recv.at[cross, step],
-                ep_at(step),
-                my_tp,
-            ).wait_recv()
+            out_copy(step, my_ep, cross).wait_recv()
             result = result + out_landed[cross, step]
-    out_ref[...] = result.astype(out_ref.dtype)
+    out_ref[...] = unfolded(result).astype(out_ref.dtype)
 
     for step in range(1, ep_size):
         feature_copy(step, my_ep, my_core, 0).wait_send()
@@ -450,9 +507,7 @@
         weight_copy(step, my_z).wait_send()
     for cross in range(CORES):
         for step in range(1 - cross, ep_size):
-            out_copy(
-                ep_at(step), other_core if cross else my_core, cross, ep_at(step)
-            ).wait_send()
+            out_copy(step, ep_at(step), cross).wait_send()
 
 
 def shards(ep_size, tp_size, features, key_table, value_table, chosen, scores):
@@ -466,13 +521,15 @@
     chunk_tokens = GROUP * own_tokens
     dma = pltpu.SemaphoreType.DMA
     slices = (z_size, own_pairs, LANES)
+    folded = (own_tokens * width // LANES, LANES)
     return pl.pallas_call(
         functools.partial(kernel, ep_size, z_size),
         out_shape=pltpu.VMEM((own_tokens, width), jnp.bfloat16),
         in_specs=[pl.BlockSpec(memory_space=pl.ANY)] * 5,
         out_specs=pl.BlockSpec(memory_space=pltpu.VMEM),
         scratch_shapes=[
-            pltpu.VMEM((CORES, tokens, width), features.dtype),
+            pltpu.VMEM((own_tokens, width), features.dtype),
+            pltpu.VMEM((CORES, ep_size) + folded, features.dtype),
             pltpu.VMEM((tokens, CORES * width), features.dtype),
             pltpu.VMEM((own_tokens, heads, top), jnp.int32),
             pltpu.VMEM((own_tokens, heads, top), jnp.float32),
@@ -486,8 +543,8 @@
             pltpu.VMEM((z_size - 1,) + slices[1:], jnp.float32),
             pltpu.VMEM(slices, jnp.bfloat16),
             pltpu.VMEM((blocks * (chunk_tokens + PITCH_PAD), LANES), jnp.float32),
-            pltpu.VMEM((CORES, tokens, width), jnp.float32),
-            pltpu.VMEM((CORES, ep_size, own_tokens, width), jnp.float32),
+            pltpu.VMEM((CORES, ep_size) + folded, jnp.float32),
+            pltpu.VMEM((CORES, ep_size) + folded, jnp.float32),
             pltpu.SemaphoreType.REGULAR,
             dma((5,)),
             dma((2,)),

time: 45 us -> 44.2 us (0.982)
  Pallas kernels: 44.3 us -> 43.5 us
    pallas_call x1, Pallas kernels: 44.3 us -> 43.5 us  [shards(): pl.pallas_call(functools.partial(kernel, ep_size, z_size), out_shape=pltp...]
where the time goes in v3:
time: 44.2 us; the launch traced here: 44.1 us
  Pallas kernels  43.5 us (98%)
  local copies, waits for them, and re-layouts  0.6 us (1%)
    pallas_call x1, Pallas kernels, shards(): pl.pallas_call(functools.partial(kernel, ep_size, z_size), out_shape=pltp...  43.5 us

profile of v3, /device:TPU:17, one launch (start us, length us, event | category | flops | bytes accessed | tf_op | source)
XLA Modules:
  0.0 44.1 jit_solution(16195083933563125589)
XLA Ops:
  0.0 43.5 %shard_map.55 = bf16[16,32]{1,0:T(8,128)(2,1)S(1)} custom-call(bf16[16,32]{1,0:T(8,128)(2,1)} %features_hbm.1, bf16[32,16384]{1,0:T(8,128)(2,1)} %bitcast.2, bf16[32,16384]{1,0:T(8,128)(2,1)} %bitcast.3, s32[16,4,16]{2,1,0:T(4,128)} %chosen_hbm.1, f32[16,4,16]{2,1,0:T(4,128)} %scores_hbm.1), custom_call_target="tpu_custom_call" | custom-call | tf_op jit(solution)/shard_map/pallas_call | solution.py:525
  43.5 0.6 %copy.7 = bf16[16,32]{1,0:T(8,128)(2,1)} copy(bf16[16,32]{1,0:T(8,128)(2,1)S(1)} %shard_map.55) | data formatting | bytes 2048

commit v4 on v3

--- a/solution.py
+++ b/solution.py
@@ -11,8 +11,11 @@
 LANES = 128
 CORES = 2
 PITCH_PAD = 4
+FIRST_GROUPS = 2
+FIRST = 2
 GROUP = 4
 LAST = 2
+CHUNK = 8
 UNROLL = 16
 MESH = pl.DeviceIdType.MESH
 
@@ -46,6 +49,7 @@
     partial,
     landed,
     weights,
+    column_hots,
     spread,
     summed,
     out_landed,
@@ -78,7 +82,6 @@
     own_pairs = own_tokens // 2
     half_rows = key.shape[1]
     blocks = half_rows // LANES
-    chunks = ep_size // GROUP
 
     side = math.isqrt(ep_size)
     folds = LANES // width
@@ -293,16 +296,18 @@
 
     steps = blocks // UNROLL
 
-    def dense_step(group, step, target):
+    def dense_step(first, size, step, target):
         rows = jnp.concatenate(
-            [features[tokens_of(far_slice(group * GROUP + inner)), :] for inner in range(GROUP)],
+            [features[tokens_of(far_slice(first + inner)), :] for inner in range(size)],
             axis=0,
         )
         columns = key[:, step * UNROLL * LANES : (step + 1) * UNROLL * LANES]
-        target[...] = jnp.dot(rows, columns, preferred_element_type=jnp.float32)
+        target[: size * own_tokens, :] = jnp.dot(
+            rows, columns, preferred_element_type=jnp.float32
+        )
 
     def take_step(step, source, found, wanted):
-        for inner in range(GROUP):
+        for inner in range(len(wanted)):
             row = wanted[inner]
             lane = row & (LANES - 1)
             block = lax.shift_right_arithmetic(row, 7)
@@ -321,23 +326,21 @@
                     found[inner],
                 )
 
-    dense_step(0, 0, dense_even)
-    pl.semaphore_wait(far_sem, 2)
-
-    def pick_group(group, carry):
-        slices = [far_slice(group * GROUP + inner) for inner in range(GROUP)]
+    buffers = (dense_even, dense_odd)
+
+    def pick_group(first, size, next_first, next_size):
+        slices = [far_slice(first + inner) for inner in range(size)]
         wanted = [picks[pairs_of(index), :] - first_row for index in slices]
-        found = [jnp.zeros((own_pairs, LANES), jnp.float32)] * GROUP
-        buffers = (dense_even, dense_odd)
+        found = [jnp.zeros((own_pairs, LANES), jnp.float32)] * size
         for step in range(steps):
             if step + 1 < steps:
-                dense_step(group, step + 1, buffers[(step + 1) % 2])
+                dense_step(first, size, step + 1, buffers[(step + 1) % 2])
             else:
-                dense_step(jnp.minimum(group + 1, chunks - 1), 0, buffers[(step + 1) % 2])
+                dense_step(next_first, next_size, 0, buffers[(step + 1) % 2])
             take_step(step, buffers[step % 2], found, wanted)
-        for inner in range(GROUP):
+        for inner in range(size):
             partial[slices[inner]] = found[inner]
-        for inner in range(GROUP):
+        for inner in range(size):
             index = slices[inner]
             step = lax.rem(index - my_z + z_size, z_size)
 
@@ -345,10 +348,50 @@
             def _():
                 part_copy(step, index).start()
 
+    dense_step(0, FIRST, 0, dense_even)
+    pl.semaphore_wait(far_sem, 2)
+
+    for group in range(FIRST_GROUPS):
+        following = (group + 1) * FIRST
+        pick_group(
+            group * FIRST,
+            FIRST,
+            following,
+            FIRST if group + 1 < FIRST_GROUPS else GROUP,
+        )
+
+    def pick_large(group, carry):
+        first = FIRST_GROUPS * FIRST + group * GROUP
+        pick_group(first, GROUP, jnp.minimum(first + GROUP, z_size - GROUP), GROUP)
         return carry
 
-    lax.fori_loop(0, chunks, pick_group, 0)
+    lax.fori_loop(0, (z_size - FIRST_GROUPS * FIRST) // GROUP, pick_large, 0)
     table_copy(1).start()
+
+    wide = own_pairs * LANES
+    pair_of = lax.shift_right_arithmetic(
+        lax.broadcasted_iota(jnp.int32, (own_pairs, wide), 1), 7
+    )
+    select = jnp.where(
+        pair_of == lax.broadcasted_iota(jnp.int32, (own_pairs, wide), 0), 1.0, 0.0
+    ).astype(jnp.bfloat16)
+    lane_numbers = lax.broadcasted_iota(jnp.int32, (LANES, LANES), 1).astype(jnp.float32)
+
+    def hot_group(group, carry):
+        for inner in range(GROUP):
+            index = group * GROUP + inner
+            lane = (picks[pairs_of(index), :] & (LANES - 1)).astype(jnp.float32)
+            wide_lane = jnp.dot(
+                lane.T.astype(jnp.bfloat16), select, preferred_element_type=jnp.float32
+            )
+            for pair in range(own_pairs):
+                column = wide_lane[:, pair * LANES : (pair + 1) * LANES]
+                column_hots[index, pair] = jnp.where(
+                    column == lane_numbers, 1.0, 0.0
+                ).astype(jnp.bfloat16)
+        return carry
+
+    lax.fori_loop(0, ep_size // GROUP, hot_group, 0)
 
     @pl.when(my_ep != my_z)
     def _():
@@ -383,7 +426,6 @@
         return jnp.where(place % 2 == 1, half, lax.rem(z_size - half, z_size))
 
     block_ids = lax.broadcasted_iota(jnp.int32, (blocks, LANES), 0)
-    lane_ids = lax.broadcasted_iota(jnp.int32, (LANES, LANES), 0)
     block_first = lax.broadcasted_iota(jnp.int32, (blocks, LANES), 1) < per_token
 
     def out_copy(step, target, cross):
@@ -397,27 +439,24 @@
             my_z * CORES + target_core,
         )
 
-    def spread_chunk(first, size):
-        quarter = fold_rows * size
-        pitch = folds * quarter + PITCH_PAD
-
-        def spread_slice(inner, carry):
-            offset = near_offset(first + inner)
-            index = z_at(offset)
+    quarter = fold_rows * CHUNK
+    pitch = folds * quarter + PITCH_PAD
+
+    def spread_group(first, place, size):
+        offsets = [near_offset(first + place + inner) for inner in range(size)]
+        for offset in offsets:
 
             @pl.when(offset != 0)
             def _():
-                weight_copy(z_size - offset, index).wait_recv()
-
+                weight_copy(z_size - offset, z_at(offset)).wait_recv()
+
+        for inner in range(size):
+            index = z_at(offsets[inner])
             slice_weights = weights[index].astype(jnp.float32)
             for pair in range(own_pairs):
                 row = picks[pl.ds(index * own_pairs + pair, 1), :] - first_row
-                weight = slice_weights[pair : pair + 1]
-                column_hot = jnp.where(
-                    (row & (LANES - 1)) == lane_ids, 1.0, 0.0
-                ).astype(jnp.bfloat16)
                 block_mask = lax.shift_right_arithmetic(row, 7) == block_ids
-                hot = jnp.where(block_mask, weight, 0.0)
+                hot = jnp.where(block_mask, slice_weights[pair : pair + 1], 0.0)
                 both = jnp.concatenate(
                     [
                         jnp.where(block_first, hot, 0.0).astype(jnp.bfloat16),
@@ -425,16 +464,17 @@
                     ],
                     axis=0,
                 )
-                placed = matmul_nt(both, column_hot)
+                placed = jnp.dot(
+                    both, column_hots[index, pair], preferred_element_type=jnp.float32
+                )
                 for half in range(2):
                     fold, row_in_fold = divmod(half * own_pairs + pair, fold_rows)
-                    place = fold * quarter + inner * fold_rows + row_in_fold
-                    spread[pl.ds(place, blocks, stride=pitch), :] = placed[
+                    target = fold * quarter + (place + inner) * fold_rows + row_in_fold
+                    spread[pl.ds(target, blocks, stride=pitch), :] = placed[
                         half * blocks : (half + 1) * blocks
                     ]
-            return carry
-
-        lax.fori_loop(0, size, spread_slice, 0)
+
+    def spread_chunk(first):
         rows = jnp.concatenate(
             [
                 spread[block * pitch : block * pitch + folds * quarter, :].astype(
@@ -445,7 +485,7 @@
             axis=1,
         )
         total = matmul_nt(rows, value[...])
-        targets = [z_at(near_offset(first + inner)) for inner in range(size)]
+        targets = [z_at(near_offset(first + inner)) for inner in range(CHUNK)]
         for core in range(CORES):
             piece = jnp.concatenate(
                 [
@@ -457,11 +497,11 @@
                 ],
                 axis=1,
             )
-            for inner in range(size):
+            for inner in range(CHUNK):
                 summed[core, targets[inner]] = piece[
                     inner * fold_rows : (inner + 1) * fold_rows
                 ]
-        for inner in range(size):
+        for inner in range(CHUNK):
             target = targets[inner]
             step = ep_step(target)
 
@@ -471,16 +511,26 @@
 
             out_copy(step, target, 1).start()
 
-    def spread_large(chunk, carry):
-        spread_chunk(chunk * GROUP, GROUP)
+    def spread_large(first, groups):
+        def step(group, carry):
+            spread_group(first, group * GROUP, GROUP)
+            return carry
+
+        lax.fori_loop(0, groups, step, 0)
+
+    def spread_small(group, carry):
+        spread_group(z_size - CHUNK, CHUNK - GROUP + group * LAST, LAST)
         return carry
 
-    def spread_small(chunk, carry):
-        spread_chunk(z_size - GROUP + chunk * LAST, LAST)
+    def spread_early(chunk, carry):
+        spread_large(chunk * CHUNK, CHUNK // GROUP)
+        spread_chunk(chunk * CHUNK)
         return carry
 
-    lax.fori_loop(0, chunks - 1, spread_large, 0)
+    lax.fori_loop(0, z_size // CHUNK - 1, spread_early, 0)
+    spread_large(z_size - CHUNK, CHUNK // GROUP - 1)
     lax.fori_loop(0, GROUP // LAST, spread_small, 0)
+    spread_chunk(z_size - CHUNK)
 
     result = summed[my_core, my_ep]
     for cross in range(CORES):
@@ -518,7 +568,7 @@
     tokens = ep_size * own_tokens
     own_pairs = own_tokens // 2
     blocks = half_rows // LANES
-    chunk_tokens = GROUP * own_tokens
+    chunk_tokens = CHUNK * own_tokens
     dma = pltpu.SemaphoreType.DMA
     slices = (z_size, own_pairs, LANES)
     folded = (own_tokens * width // LANES, LANES)
@@ -537,11 +587,12 @@
             pltpu.VMEM((own_pairs, LANES), jnp.float32),
             pltpu.VMEM((CORES * width, half_rows), key_table.dtype),
             pltpu.VMEM((CORES * width, half_rows), value_table.dtype),
-            pltpu.VMEM((chunk_tokens, UNROLL * LANES), jnp.float32),
-            pltpu.VMEM((chunk_tokens, UNROLL * LANES), jnp.float32),
+            pltpu.VMEM((GROUP * own_tokens, UNROLL * LANES), jnp.float32),
+            pltpu.VMEM((GROUP * own_tokens, UNROLL * LANES), jnp.float32),
             pltpu.VMEM(slices, jnp.float32),
             pltpu.VMEM((z_size - 1,) + slices[1:], jnp.float32),
             pltpu.VMEM(slices, jnp.bfloat16),
+            pltpu.VMEM((ep_size, own_pairs, LANES, LANES), jnp.bfloat16),
             pltpu.VMEM((blocks * (chunk_tokens + PITCH_PAD), LANES), jnp.float32),
             pltpu.VMEM((CORES, ep_size) + folded, jnp.float32),
             pltpu.VMEM((CORES, ep_size) + folded, jnp.float32),

time: 44.2 us -> 42.3 us (0.957)
  Pallas kernels: 43.5 us -> 41.6 us
    pallas_call x1, Pallas kernels: 43.5 us -> 41.6 us  [shards(): pl.pallas_call(functools.partial(kernel, ep_size, z_size), out_shape=pltp...]
where the time goes in v4:
time: 42.3 us; the launch traced here: 42.2 us
  Pallas kernels  41.6 us (98%)
  local copies, waits for them, and re-layouts  0.6 us (1%)
    pallas_call x1, Pallas kernels, shards(): pl.pallas_call(functools.partial(kernel, ep_size, z_size), out_shape=pltp...  41.6 us

profile of v4, /device:TPU:17, one launch (start us, length us, event | category | flops | bytes accessed | tf_op | source)
XLA Modules:
  0.0 42.2 jit_solution(7019536574074896752)
XLA Ops:
  0.0 41.6 %shard_map.55 = bf16[16,32]{1,0:T(8,128)(2,1)S(1)} custom-call(bf16[16,32]{1,0:T(8,128)(2,1)} %features_hbm.1, bf16[32,16384]{1,0:T(8,128)(2,1)} %bitcast.2, bf16[32,16384]{1,0:T(8,128)(2,1)} %bitcast.3, s32[16,4,16]{2,1,0:T(4,128)} %chosen_hbm.1, f32[16,4,16]{2,1,0:T(4,128)} %scores_hbm.1), custom_call_target="tpu_custom_call" | custom-call | tf_op jit(solution)/shard_map/pallas_call | solution.py:575
  41.6 0.6 %copy.7 = bf16[16,32]{1,0:T(8,128)(2,1)} copy(bf16[16,32]{1,0:T(8,128)(2,1)S(1)} %shard_map.55) | data formatting | bytes 2048

commit v5 on v4

--- a/solution.py
+++ b/solution.py
@@ -53,6 +53,7 @@
     spread,
     summed,
     out_landed,
+    middle_sem,
     far_sem,
     local_sem,
     table_send,
@@ -140,24 +141,26 @@
         table_copies.append(copy)
 
     barrier = pltpu.get_barrier_semaphore()
-    reach = z_size // 4
+    near, middle = z_size // 8, z_size // 4
 
     def greet(ep, tp):
         pl.semaphore_signal(barrier, inc=1, device_id=(ep, tp), device_id_type=MESH)
 
-    for step in far_first:
-        greet(ep_at(step), my_tp)
-        greet(ep_at(step), partner)
-        if step <= reach:
-            greet(my_ep, z_at(reach + 1 - step) * CORES + my_core)
-            greet(my_ep, z_at(z_size - reach - 1 + step) * CORES + my_core)
+    lines = sorted(range(1, side), key=hops, reverse=True)
+    for line in lines:
+        greet(ep_at(line), my_tp)
+        greet(ep_at(line), partner)
+        greet(ep_at(line * side), my_tp)
+    for step in range(near, 0, -1):
+        greet(my_ep, z_at(step) * CORES + my_core)
+        greet(my_ep, z_at(z_size - step) * CORES + my_core)
     greet(my_ep, partner)
 
     for copy in small_copies:
         copy.wait()
 
     tokens_here = own_features[...].astype(jnp.float32)
-    feature_parts[my_core, my_ep] = jnp.concatenate(
+    feature_parts[my_ep, my_core] = jnp.concatenate(
         [tokens_here[fold * fold_rows : (fold + 1) * fold_rows] for fold in range(folds)],
         axis=1,
     ).astype(jnp.bfloat16)
@@ -182,14 +185,18 @@
     def _():
         gates[...] = packed(gate_pieces)
 
-    pl.semaphore_wait(barrier, 2 * reach + CORES * (ep_size - 1) + 1)
-    for step in (reach, z_size - reach):
-        pl.semaphore_signal(
-            far_sem,
-            inc=1,
-            device_id=(my_ep, z_at(step) * CORES + my_core),
-            device_id_type=MESH,
-        )
+    pl.semaphore_wait(barrier, 3 * (side - 1) + 2 * near + 1)
+
+    def tell(semaphore, distance):
+        for step in (distance, z_size - distance):
+            pl.semaphore_signal(
+                semaphore,
+                inc=1,
+                device_id=(my_ep, z_at(step) * CORES + my_core),
+                device_id_type=MESH,
+            )
+
+    tell(middle_sem, near)
 
     def remote(source, target, send, recv, ep, tp):
         return pltpu.make_async_remote_copy(
@@ -201,22 +208,41 @@
             device_id_type=MESH,
         )
 
-    def pick_copy(step, owner):
+    def pick_copy(line, owner):
         slot = picks.at[pairs_of(owner)]
         return remote(
-            slot, slot, pick_send.at[step - 1], pick_recv.at[step - 1], ep_at(step), my_tp
-        )
-
-    def feature_copy(step, owner, source_core, cross):
-        slot = feature_parts.at[source_core, owner]
+            slot, slot, pick_send.at[0, line], pick_recv.at[0, line], ep_at(line), my_tp
+        )
+
+    def feature_copy(line, owner, source_core, cross):
+        slot = feature_parts.at[owner, source_core]
         return remote(
             slot,
             slot,
-            feature_send.at[cross, step],
-            feature_recv.at[cross, step],
-            ep_at(step),
+            feature_send.at[cross, line],
+            feature_recv.at[cross, line],
+            ep_at(line),
             partner if cross else my_tp,
         )
+
+    def row_copies(line, owner):
+        row = owner // side
+        row_pairs = side * own_pairs
+        copies = []
+        for slot, send, recv in (
+            (
+                feature_parts.at[pl.ds(row * side, side)],
+                feature_send.at[CORES, line],
+                feature_recv.at[CORES, line],
+            ),
+            (
+                picks.at[pl.ds(pl.multiple_of(row * row_pairs, row_pairs), row_pairs)],
+                pick_send.at[1, line],
+                pick_recv.at[1, line],
+            ),
+        ):
+            copies.append(remote(slot, slot, send, recv, ep_at(line * side), my_tp))
+        return copies
 
     def gate_copy(step):
         return remote(
@@ -234,32 +260,34 @@
             partner,
         )
 
-    for step in far_first:
-        feature_copy(step, my_ep, my_core, 0).start()
-        feature_copy(step, my_ep, my_core, 1).start()
-        pick_copy(step, my_ep).start()
+    for line in lines:
+        feature_copy(line, my_ep, my_core, 0).start()
+        feature_copy(line, my_ep, my_core, 1).start()
+        pick_copy(line, my_ep).start()
     feature_copy(0, my_ep, my_core, 1).start()
     table_copy(0).start()
 
-    @pl.when(my_ep == my_z)
-    def _():
-        for step in far_first:
-            gate_copy(step).start()
-
-    for step in range(1, ep_size):
-        feature_copy(step, source_ep(step), my_core, 0).wait_recv()
-    for step in range(ep_size):
-        feature_copy(step, source_ep(step), other_core, 1).wait_recv()
+    feature_copy(0, my_ep, other_core, 1).wait_recv()
+    for line in lines:
+        feature_copy(line, source_ep(line), my_core, 0).wait_recv()
+        feature_copy(line, source_ep(line), other_core, 1).wait_recv()
+        pick_copy(line, source_ep(line)).wait_recv()
+    for line in lines:
+        for copy in row_copies(line, my_ep):
+            copy.start()
+    pl.semaphore_wait(middle_sem, 2)
+    tell(far_sem, middle)
+    for line in lines:
+        for copy in row_copies(line, source_ep(line * side)):
+            copy.wait_recv()
     for owner in range(ep_size):
         features[owner * own_tokens : (owner + 1) * own_tokens, :] = jnp.concatenate(
             [
-                unfolded(feature_parts[core, owner].astype(jnp.float32))
+                unfolded(feature_parts[owner, core].astype(jnp.float32))
                 for core in range(CORES)
             ],
             axis=1,
         ).astype(jnp.bfloat16)
-    for step in range(1, ep_size):
-        pick_copy(step, source_ep(step)).wait_recv()
     table_copies[0].wait()
 
     def table_landed(number):
@@ -359,6 +387,11 @@
             following,
             FIRST if group + 1 < FIRST_GROUPS else GROUP,
         )
+
+    @pl.when(my_ep == my_z)
+    def _():
+        for step in far_first:
+            gate_copy(step).start()
 
     def pick_large(group, carry):
         first = FIRST_GROUPS * FIRST + group * GROUP
@@ -539,10 +572,12 @@
             result = result + out_landed[cross, step]
     out_ref[...] = unfolded(result).astype(out_ref.dtype)
 
-    for step in range(1, ep_size):
-        feature_copy(step, my_ep, my_core, 0).wait_send()
-        feature_copy(step, my_ep, my_core, 1).wait_send()
-        pick_copy(step, my_ep).wait_send()
+    for line in lines:
+        feature_copy(line, my_ep, my_core, 0).wait_send()
+        feature_copy(line, my_ep, my_core, 1).wait_send()
+        pick_copy(line, my_ep).wait_send()
+        for copy in row_copies(line, my_ep):
+            copy.wait_send()
     feature_copy(0, my_ep, my_core, 1).wait_send()
 
     @pl.when(my_ep == my_z)
@@ -570,6 +605,7 @@
     blocks = half_rows // LANES
     chunk_tokens = CHUNK * own_tokens
     dma = pltpu.SemaphoreType.DMA
+    side = math.isqrt(ep_size)
     slices = (z_size, own_pairs, LANES)
     folded = (own_tokens * width // LANES, LANES)
     return pl.pallas_call(
@@ -579,7 +615,7 @@
         out_specs=pl.BlockSpec(memory_space=pltpu.VMEM),
         scratch_shapes=[
             pltpu.VMEM((own_tokens, width), features.dtype),
-            pltpu.VMEM((CORES, ep_size) + folded, features.dtype),
+            pltpu.VMEM((ep_size, CORES) + folded, features.dtype),
             pltpu.VMEM((tokens, CORES * width), features.dtype),
             pltpu.VMEM((own_tokens, heads, top), jnp.int32),
             pltpu.VMEM((own_tokens, heads, top), jnp.float32),
@@ -597,13 +633,14 @@
             pltpu.VMEM((CORES, ep_size) + folded, jnp.float32),
             pltpu.VMEM((CORES, ep_size) + folded, jnp.float32),
             pltpu.SemaphoreType.REGULAR,
+            pltpu.SemaphoreType.REGULAR,
             dma((5,)),
             dma((2,)),
             dma((2,)),
-            dma((CORES, ep_size)),
-            dma((CORES, ep_size)),
-            dma((ep_size - 1,)),
-            dma((ep_size - 1,)),
+            dma((CORES + 1, side)),
+            dma((CORES + 1, side)),
+            dma((2, side)),
+            dma((2, side)),
             dma((ep_size - 1,)),
             dma((1,)),
             dma((z_size - 1,)),

time: 42.3 us -> 43 us (1.017)
  Pallas kernels: 41.6 us -> 42.3 us
    pallas_call x1, Pallas kernels: 41.6 us -> 42.3 us  [shards(): pl.pallas_call(functools.partial(kernel, ep_size, z_size), out_shape=pltp...]
where the time goes in v5:
time: 43 us; the launch traced here: 42.9 us
  Pallas kernels  42.3 us (98%)
  local copies, waits for them, and re-layouts  0.6 us (1%)
    pallas_call x1, Pallas kernels, shards(): pl.pallas_call(functools.partial(kernel, ep_size, z_size), out_shape=pltp...  42.3 us

profile of v5, /device:TPU:17, one launch (start us, length us, event | category | flops | bytes accessed | tf_op | source)
XLA Modules:
  0.0 42.9 jit_solution(7026116788717752166)
XLA Ops:
  0.0 42.3 %shard_map.55 = bf16[16,32]{1,0:T(8,128)(2,1)S(1)} custom-call(bf16[16,32]{1,0:T(8,128)(2,1)} %features_hbm.1, bf16[32,16384]{1,0:T(8,128)(2,1)} %bitcast.2, bf16[32,16384]{1,0:T(8,128)(2,1)} %bitcast.3, s32[16,4,16]{2,1,0:T(4,128)} %chosen_hbm.1, f32[16,4,16]{2,1,0:T(4,128)} %scores_hbm.1), custom_call_target="tpu_custom_call" | custom-call | tf_op jit(solution)/shard_map/pallas_call | solution.py:611
  42.3 0.6 %copy.7 = bf16[16,32]{1,0:T(8,128)(2,1)} copy(bf16[16,32]{1,0:T(8,128)(2,1)S(1)} %shard_map.55) | data formatting | bytes 2048

commit v6 on v4

--- a/solution.py
+++ b/solution.py
@@ -11,11 +11,8 @@
 LANES = 128
 CORES = 2
 PITCH_PAD = 4
-FIRST_GROUPS = 2
-FIRST = 2
-GROUP = 4
-LAST = 2
-CHUNK = 8
+GROUP = 2
+CHUNK = 4
 UNROLL = 16
 MESH = pl.DeviceIdType.MESH
 
@@ -296,18 +293,16 @@
 
     steps = blocks // UNROLL
 
-    def dense_step(first, size, step, target):
+    def dense_step(first, step, target):
         rows = jnp.concatenate(
-            [features[tokens_of(far_slice(first + inner)), :] for inner in range(size)],
+            [features[tokens_of(far_slice(first + inner)), :] for inner in range(GROUP)],
             axis=0,
         )
         columns = key[:, step * UNROLL * LANES : (step + 1) * UNROLL * LANES]
-        target[: size * own_tokens, :] = jnp.dot(
-            rows, columns, preferred_element_type=jnp.float32
-        )
+        target[...] = jnp.dot(rows, columns, preferred_element_type=jnp.float32)
 
     def take_step(step, source, found, wanted):
-        for inner in range(len(wanted)):
+        for inner in range(GROUP):
             row = wanted[inner]
             lane = row & (LANES - 1)
             block = lax.shift_right_arithmetic(row, 7)
@@ -328,19 +323,21 @@
 
     buffers = (dense_even, dense_odd)
 
-    def pick_group(first, size, next_first, next_size):
-        slices = [far_slice(first + inner) for inner in range(size)]
+    def pick_group(group, carry):
+        first = group * GROUP
+        following = jnp.minimum(first + GROUP, z_size - GROUP)
+        slices = [far_slice(first + inner) for inner in range(GROUP)]
         wanted = [picks[pairs_of(index), :] - first_row for index in slices]
-        found = [jnp.zeros((own_pairs, LANES), jnp.float32)] * size
+        found = [jnp.zeros((own_pairs, LANES), jnp.float32)] * GROUP
         for step in range(steps):
             if step + 1 < steps:
-                dense_step(first, size, step + 1, buffers[(step + 1) % 2])
+                dense_step(first, step + 1, buffers[(step + 1) % 2])
             else:
-                dense_step(next_first, next_size, 0, buffers[(step + 1) % 2])
+                dense_step(following, 0, buffers[(step + 1) % 2])
             take_step(step, buffers[step % 2], found, wanted)
-        for inner in range(size):
+        for inner in range(GROUP):
             partial[slices[inner]] = found[inner]
-        for inner in range(size):
+        for inner in range(GROUP):
             index = slices[inner]
             step = lax.rem(index - my_z + z_size, z_size)
 
@@ -348,24 +345,11 @@
             def _():
                 part_copy(step, index).start()
 
-    dense_step(0, FIRST, 0, dense_even)
+        return carry
+
+    dense_step(0, 0, dense_even)
     pl.semaphore_wait(far_sem, 2)
-
-    for group in range(FIRST_GROUPS):
-        following = (group + 1) * FIRST
-        pick_group(
-            group * FIRST,
-            FIRST,
-            following,
-            FIRST if group + 1 < FIRST_GROUPS else GROUP,
-        )
-
-    def pick_large(group, carry):
-        first = FIRST_GROUPS * FIRST + group * GROUP
-        pick_group(first, GROUP, jnp.minimum(first + GROUP, z_size - GROUP), GROUP)
-        return carry
-
-    lax.fori_loop(0, (z_size - FIRST_GROUPS * FIRST) // GROUP, pick_large, 0)
+    lax.fori_loop(0, z_size // GROUP, pick_group, 0)
     table_copy(1).start()
 
     wide = own_pairs * LANES
@@ -442,15 +426,15 @@
     quarter = fold_rows * CHUNK
     pitch = folds * quarter + PITCH_PAD
 
-    def spread_group(first, place, size):
-        offsets = [near_offset(first + place + inner) for inner in range(size)]
+    def spread_group(first, place):
+        offsets = [near_offset(first + place + inner) for inner in range(GROUP)]
         for offset in offsets:
 
             @pl.when(offset != 0)
             def _():
                 weight_copy(z_size - offset, z_at(offset)).wait_recv()
 
-        for inner in range(size):
+        for inner in range(GROUP):
             index = z_at(offsets[inner])
             slice_weights = weights[index].astype(jnp.float32)
             for pair in range(own_pairs):
@@ -511,26 +495,16 @@
 
             out_copy(step, target, 1).start()
 
-    def spread_large(first, groups):
-        def step(group, carry):
-            spread_group(first, group * GROUP, GROUP)
-            return carry
-
-        lax.fori_loop(0, groups, step, 0)
-
-    def spread_small(group, carry):
-        spread_group(z_size - CHUNK, CHUNK - GROUP + group * LAST, LAST)
-        return carry
-
-    def spread_early(chunk, carry):
-        spread_large(chunk * CHUNK, CHUNK // GROUP)
+    def spread_step(chunk, carry):
+        def step(group, inner_carry):
+            spread_group(chunk * CHUNK, group * GROUP)
+            return inner_carry
+
+        lax.fori_loop(0, CHUNK // GROUP, step, 0)
         spread_chunk(chunk * CHUNK)
         return carry
 
-    lax.fori_loop(0, z_size // CHUNK - 1, spread_early, 0)
-    spread_large(z_size - CHUNK, CHUNK // GROUP - 1)
-    lax.fori_loop(0, GROUP // LAST, spread_small, 0)
-    spread_chunk(z_size - CHUNK)
+    lax.fori_loop(0, z_size // CHUNK, spread_step, 0)
 
     result = summed[my_core, my_ep]
     for cross in range(CORES):

time: 42.3 us -> 41.6 us (0.983)
  Pallas kernels: 41.6 us -> 40.9 us
    pallas_call x1, Pallas kernels: 41.6 us -> 40.9 us  [shards(): pl.pallas_call(functools.partial(kernel, ep_size, z_size), out_shape=pltp...]
where the time goes in v6:
time: 41.6 us; the launch traced here: 41.5 us
  Pallas kernels  40.9 us (98%)
  local copies, waits for them, and re-layouts  0.6 us (1%)
    pallas_call x1, Pallas kernels, shards(): pl.pallas_call(functools.partial(kernel, ep_size, z_size), out_shape=pltp...  40.9 us

profile of v6, /device:TPU:17, one launch (start us, length us, event | category | flops | bytes accessed | tf_op | source)
XLA Modules:
  0.0 41.5 jit_solution(4735871308360310480)
XLA Ops:
  0.0 40.9 %shard_map.55 = bf16[16,32]{1,0:T(8,128)(2,1)S(1)} custom-call(bf16[16,32]{1,0:T(8,128)(2,1)} %features_hbm.1, bf16[32,16384]{1,0:T(8,128)(2,1)} %bitcast.2, bf16[32,16384]{1,0:T(8,128)(2,1)} %bitcast.3, s32[16,4,16]{2,1,0:T(4,128)} %chosen_hbm.1, f32[16,4,16]{2,1,0:T(4,128)} %scores_hbm.1), custom_call_target="tpu_custom_call" | custom-call | tf_op jit(solution)/shard_map/pallas_call | solution.py:549
  40.9 0.6 %copy.7 = bf16[16,32]{1,0:T(8,128)(2,1)} copy(bf16[16,32]{1,0:T(8,128)(2,1)S(1)} %shard_map.55) | data formatting | bytes 2048

commit v7 on v6

--- a/solution.py
+++ b/solution.py
@@ -142,12 +142,12 @@
     def greet(ep, tp):
         pl.semaphore_signal(barrier, inc=1, device_id=(ep, tp), device_id_type=MESH)
 
+    for step in range(reach, 0, -1):
+        greet(my_ep, z_at(step) * CORES + my_core)
+        greet(my_ep, z_at(z_size - step) * CORES + my_core)
     for step in far_first:
         greet(ep_at(step), my_tp)
         greet(ep_at(step), partner)
-        if step <= reach:
-            greet(my_ep, z_at(reach + 1 - step) * CORES + my_core)
-            greet(my_ep, z_at(z_size - reach - 1 + step) * CORES + my_core)
     greet(my_ep, partner)
 
     for copy in small_copies:
@@ -234,6 +234,7 @@
     for step in far_first:
         feature_copy(step, my_ep, my_core, 0).start()
         feature_copy(step, my_ep, my_core, 1).start()
+    for step in far_first:
         pick_copy(step, my_ep).start()
     feature_copy(0, my_ep, my_core, 1).start()
     table_copy(0).start()

time: 41.6 us -> 41.7 us (level)
  no operation moved by 1% of the time
where the time goes in v7:
time: 41.7 us; the launch traced here: 41.6 us
  Pallas kernels  41 us (98%)
  local copies, waits for them, and re-layouts  0.6 us (1%)
    pallas_call x1, Pallas kernels, shards(): pl.pallas_call(functools.partial(kernel, ep_size, z_size), out_shape=pltp...  41 us

profile of v7, /device:TPU:17, one launch (start us, length us, event | category | flops | bytes accessed | tf_op | source)
XLA Modules:
  0.0 41.6 jit_solution(10193237501478273381)
XLA Ops:
  0.0 41.0 %shard_map.55 = bf16[16,32]{1,0:T(8,128)(2,1)S(1)} custom-call(bf16[16,32]{1,0:T(8,128)(2,1)} %features_hbm.1, bf16[32,16384]{1,0:T(8,128)(2,1)} %bitcast.2, bf16[32,16384]{1,0:T(8,128)(2,1)} %bitcast.3, s32[16,4,16]{2,1,0:T(4,128)} %chosen_hbm.1, f32[16,4,16]{2,1,0:T(4,128)} %scores_hbm.1), custom_call_target="tpu_custom_call" | custom-call | tf_op jit(solution)/shard_map/pallas_call | solution.py:550
  41.0 0.6 %copy.7 = bf16[16,32]{1,0:T(8,128)(2,1)} copy(bf16[16,32]{1,0:T(8,128)(2,1)S(1)} %shard_map.55) | data formatting | bytes 2048
